TPU v7x, 32 devices: a whole 2x2x4 slice. The times are simulated.
32 devices in a mesh: gr: 2 (over x), sp: 8 (over z, y), tp: 2 (over core).
Axes of the slice: x: 2, y: 2, z: 4, core: 2. Of those that a mesh axis runs over, the one named last changes fastest.
Arguments:
- tokens: bfloat16 [8, 2048, 2048], P('gr', 'sp'), parts along dimension 0, may hold values from -6 to 6
- new_rows: bfloat16 [8, 2048], P('gr'), parts along dimension 0, may hold values from -6 to 6
- new_query: bfloat16 [8, 1024], P('gr', 'tp'), parts along dimension 0, may hold values from -6 to 6
- norm_gain: bfloat16 [2048], replicated, may hold values from 0.099609375 to 1.8984375
- key_weight: bfloat16 [2048, 1024], P('sp', 'tp'), may hold values from -0.125 to 0.125
- value_weight: bfloat16 [2048, 2048], P('sp', 'tp'), may hold values from -0.125 to 0.125
- input_weight: bfloat16 [2048, 16], replicated, may hold values from -0.125 to 0.125
- forget_weight: bfloat16 [2048, 16], replicated, may hold values from -0.125 to 0.125
- forget_bias: float32 [16], P('tp'), may hold values from 3 to 12
- gate_offsets: float32 [8, 2048, 2, 16], P('gr', 'sp', None, 'tp'), parts along dimension 0, may hold values from -6 to 250, as said below
Outputs:
- cache_keys: bfloat16 [16, 1024, 1024], P(('gr', 'sp'), None, 'tp'), parts along dimension 0
- cache_values: bfloat16 [16, 1024, 2048], P(('gr', 'sp'), None, 'tp'), parts along dimension 0
- cache_weights: float32 [16, 16, 1024], P(('gr', 'sp'), 'tp'), parts along dimension 0
- first_read: bfloat16 [8, 2048], P('gr', 'tp'), parts along dimension 0
There are 2 independent parts, one for each index of `gr`. A program takes and returns all parts, laid end to end along the dimension named above; an argument that names none is the same for every part. Nothing has to cross between parts.
Inputs may be any that keep to these rules, and one draw needn't show every extreme that they name: `gate_offsets`: entry 1 along the third dimension is never positive.
All inputs are finite; a program needn't handle non-finite values.
Results may differ from a plain program's by a relative error of at most 0.012.
The roundings to bfloat16 on the way count: a program that leaves them out, or rounds other values in their place, can miss the bound.
Values may be sent and summed in bfloat16 or wider, within the bound.
A program may use at most 64 MiB of HBM per device.

v0:
```python
import jax
import jax.numpy as jnp
from jax import lax
from jax.sharding import PartitionSpec as P

EPSILON = 1e-06
HIGHEST = lax.Precision.HIGHEST


def normed_rows(source, norm_gain):
    widened = source.astype(jnp.float32)
    inverse_rms = lax.rsqrt(jnp.mean(widened * widened, axis=-1, keepdims=True) + EPSILON)
    return (widened * inverse_rms * norm_gain.astype(jnp.float32)).astype(jnp.bfloat16)


def contract_last(a, b):
    return lax.dot_general(a, b, (((1,), (1,)), ((), ())), preferred_element_type=jnp.float32)


def log_weights(gates, offsets, forget_bias, heads, blocks, pieces):
    rows = gates.shape[1]
    sub = rows // blocks
    input_gate = gates[:heads] + offsets[:heads]
    log_forget = jax.nn.log_sigmoid(gates[heads:] + forget_bias[:, None]) + offsets[heads:]
    by_block = log_forget.reshape(heads, blocks, sub)
    later = jnp.tril(jnp.ones((sub, sub), jnp.float32), -1)
    within = jnp.dot(by_block.reshape(heads * blocks, sub), later, precision=HIGHEST)
    totals = jnp.sum(by_block, axis=2)
    index = lax.axis_index("sp")
    everything = lax.all_gather(totals, "sp")
    ours = lax.dynamic_slice_in_dim(everything, index // pieces * pieces, pieces, 0)
    piece = index % pieces
    all_pieces = jnp.sum(ours, axis=0)
    after = jnp.flip(jnp.cumsum(jnp.flip(all_pieces, 1), axis=1), 1) - all_pieces
    follows = (jnp.arange(pieces) > piece).astype(jnp.float32)
    after = after + jnp.sum(ours * follows[:, None, None], axis=0)
    suffix = within.reshape(heads, blocks, sub) + after[:, :, None]
    return input_gate + suffix.reshape(heads, rows)


def read_part(query, keys, values, log_weight, heads):
    key_size = keys.shape[1] // heads
    value_size = values.shape[1] // heads
    peak = jnp.max(log_weight, axis=1, keepdims=True)
    own_head = jnp.arange(heads)[:, None] == jnp.arange(keys.shape[1])[None, :] // key_size
    spread = jnp.where(own_head, query, jnp.zeros_like(query))
    scores = contract_last(spread, keys)
    terms = jnp.exp(log_weight - peak) * scores
    wide = jnp.dot(terms.astype(jnp.bfloat16), values, preferred_element_type=jnp.float32)
    pick = jnp.eye(heads, dtype=jnp.float32)
    numerator = jnp.sum(wide.reshape(heads, heads, value_size) * pick[:, :, None], axis=1)
    return (peak, numerator, jnp.sum(terms, axis=1, keepdims=True))


def finish(peak, numerator, denominator, own_score, gate_new, value_new, seq_count, pieces):
    heads, value_size = numerator.shape
    one = jnp.concatenate([peak, denominator, own_score, gate_new], axis=1)
    one = jnp.pad(one, ((0, 0), (0, value_size - one.shape[1])))
    packed = jnp.concatenate([numerator, value_new, one], axis=1)
    everything = lax.all_gather(packed, "sp").reshape(seq_count, pieces, heads, -1)
    one = everything[..., 2 * value_size :]
    peaks, denominators = (one[..., 0], one[..., 1])
    own_score, gate_new = (one[:, 0, :, 2], one[:, 0, :, 3])
    value_new = everything[:, 0, :, value_size : 2 * value_size]
    top = jnp.maximum(jnp.max(peaks, axis=1), gate_new)
    old = jnp.exp(peaks - top[:, None])
    new = jnp.exp(gate_new - top) * own_score
    total = jnp.sum(old[..., None] * everything[..., :value_size], axis=1)
    total = total + new[..., None] * value_new
    weight = jnp.sum(old * denominators, axis=1) + new
    return total / jnp.maximum(jnp.abs(weight), 1.0)[..., None]


def per_device(
    tokens,
    new_rows,
    new_query,
    norm_gain,
    key_weight,
    value_weight,
    input_weight,
    forget_weight,
    forget_bias,
    gate_offsets,
):
    seq_count, positions, model_width = tokens.shape
    heads = forget_bias.shape[0]
    key_size = key_weight.shape[1] // heads
    group = lax.axis_size("sp")
    shares = lax.axis_size("tp")
    pieces = group // seq_count
    sub = positions // pieces
    rows = group * sub
    index, core = (lax.axis_index("sp"), lax.axis_index("tp"))
    prompt = index // pieces
    part = model_width // shares
    mine = lax.dynamic_slice_in_dim(tokens.reshape(group, sub, model_width), core * part, part, 2)
    moved = lax.all_to_all(mine, "sp", split_axis=0, concat_axis=0, tiled=True)
    source = lax.all_gather(moved.reshape(rows, part), "tp", axis=1, tiled=True)
    offsets = jnp.transpose(gate_offsets.reshape(group, sub, 2 * heads), (0, 2, 1))
    offsets = lax.all_to_all(offsets, "sp", split_axis=0, concat_axis=0, tiled=True)
    offsets = jnp.transpose(offsets, (1, 0, 2)).reshape(2 * heads, rows)
    key_weight = lax.all_gather(key_weight, "sp", axis=0, tiled=True)
    value_weight = lax.all_gather(value_weight, "sp", axis=0, tiled=True)
    normed = normed_rows(source, norm_gain)
    fresh = normed_rows(lax.dynamic_slice_in_dim(new_rows, prompt, 1, 0), norm_gain)
    head_start = core * heads
    gate_weight = jnp.concatenate(
        [
            lax.dynamic_slice_in_dim(input_weight, head_start, heads, 1),
            lax.dynamic_slice_in_dim(forget_weight, head_start, heads, 1),
        ],
        axis=1,
    ).T
    gates = contract_last(gate_weight, normed)
    gate_new = contract_last(gate_weight[:heads], fresh)

    def project(x):
        keys = jnp.dot(x, key_weight, preferred_element_type=jnp.float32) * key_size ** (-0.5)
        values = jnp.dot(x, value_weight, preferred_element_type=jnp.float32)
        return (keys.astype(jnp.bfloat16), values.astype(jnp.bfloat16))

    keys, values = project(normed)
    key_new, value_new = project(fresh)
    log_weight = log_weights(gates, offsets, forget_bias, heads, group, pieces)
    query = lax.dynamic_slice_in_dim(new_query, prompt, 1, 0)
    peak, numerator, denominator = read_part(query, keys, values, log_weight, heads)
    own_score = jnp.sum(
        (query.astype(jnp.float32) * key_new.astype(jnp.float32)).reshape(heads, key_size),
        axis=1,
        keepdims=True,
    )
    value_new = value_new.astype(jnp.float32).reshape(heads, -1)
    read_out = finish(
        peak, numerator, denominator, own_score, gate_new, value_new, seq_count, pieces
    )
    return (
        keys[None],
        values[None],
        log_weight[None],
        read_out.reshape(seq_count, -1).astype(jnp.bfloat16),
    )


def solution(mesh):
    return jax.shard_map(
        per_device,
        mesh=mesh,
        in_specs=(
            P("gr", "sp", None),
            P("gr", None),
            P("gr", "tp"),
            P(),
            P("sp", "tp"),
            P("sp", "tp"),
            P(),
            P(),
            P("tp"),
            P("gr", "sp", None, "tp"),
        ),
        out_specs=(
            P(("gr", "sp"), None, "tp"),
            P(("gr", "sp"), None, "tp"),
            P(("gr", "sp"), "tp", None),
            P("gr", "tp"),
        ),
        check_vma=False,
    )
```

profile of v0, /device:TPU:0, one launch (start us, length us, event | category | flops | bytes accessed | tf_op | source)
XLA Modules:
  0.0 263.4 jit_solution(13032726843708910737)
XLA Ops:
  7.2 0.7 all-gather.8.cloned.1.call-update
  7.9 0.7 all-gather.10.cloned.1.call-update
  8.7 1.8 constant_dynamic-slice_fusion.4
  10.5 80.9 %all_to_all.10 = bf16[8,128,1024]{2,1,0:T(8,128)(2,1)} all-to-all(bf16[8,128,1024]{2,1,0:T(8,128)(2,1)S(1)} %constant_dynamic-slice_fusion.4), channel_id=1, replica_groups=mesh['gr'=2,'sp'=8,'tp'=2] {'sp'}, dimensions={0} | all-to-all | bytes 4194304 | tf_op jit(solution)/shard_map/all_to_all | solution.py:98
  91.5 0.6 copy.36
  92.2 3.6 %all-to-all-start.1 = ((f32[8,16,128]{2,1,0:T(8,128)}), f32[8,16,128]{2,1,0:T(8,128)S(1)}, u32[]{:S(2)}, u32[]{:S(2)}) async-start(f32[8,16,128]{2,1,0:T(8,128)} %copy.36), calls=%async_computation.1 | async-start | bytes 131072 | tf_op jit(solution)/shard_map/all_to_all | solution.py:101
  95.8 0.6 multiply_reduce_fusion
  97.3 0.1 convolution_bitcast_fusion.1
  97.4 2.0 fusion.27
  99.5 0.1 reduce_sum.99
  99.6 0.1 copy.43
  99.7 61.1 %all-gather.10.cloned.1.call-done = bf16[2048,1024]{1,0:T(8,128)(2,1)} async-done(((bf16[256,1024]{1,0:T(8,128)(2,1)}), bf16[2048,1024]{1,0:T(8,128)(2,1)}) %all-gather.10.cloned.1.call-update) | async-done | bytes 4194320 | tf_op jit(solution)/shard_map/all_gather | solution.py:104
  160.8 2.8 %fusion.29 = f32[1,1024]{1,0:T(1,128)S(1)} fusion(bf16[2048,1024]{1,0:T(8,128)(2,1)} %all-gather.10.cloned.1.call-done, bf16[1,2048]{1,0:T(2,128)(2,1)S(1)} %multiply_multiply_fusion), kind=kOutput, calls=%fused_computation.55 | convolution fusion | flops 4194304 | bytes 4202496 | tf_op jit(solution)/shard_map/dot_general | solution.py:120
  163.6 10.9 %all-gather.6.cloned.1.call-done = bf16[1024,2048]{1,0:T(8,128)(2,1)} async-done(((bf16[1024,1024]{1,0:T(8,128)(2,1)}), bf16[1024,2048]{1,0:T(8,128)(2,1)}) %all-gather.6.cloned.1.call-update) | async-done | bytes 4194320 | tf_op jit(solution)/shard_map/all_gather | solution.py:99
  174.6 3.2 %fusion = f32[1024]{0:T(1024)S(1)} fusion(bf16[1024,2048]{1,0:T(8,128)(2,1)} %all-gather.6.cloned.1.call-done), kind=kLoop, calls=%fused_computation.2 | loop fusion | flops 6290432 | bytes 4198400 | tf_op jit(solution)/shard_map/reduce_sum | solution.py:12
  177.8 0.2 copy-done
  178.0 1.3 fusion.9
  179.3 0.2 fusion.52
  179.5 30.9 %all-gather = f32[64,8]{1,0:T(8,128)S(1)} all-gather(f32[8,8]{1,0:T(8,128)S(1)} %copy.38), channel_id=2, replica_groups=mesh['gr'=2,'sp'=8,'tp'=2] {'sp'}, dimensions={0}, use_global_device_ids=true | all-gather | bytes 2304 | tf_op jit(solution)/shard_map/all_gather | solution.py:30
  210.7 0.1 multiply_reduce_fusion.1
  210.9 0.3 fusion.4
  211.1 0.1 fusion.50
  211.3 0.1 copy.41
  211.3 4.6 %multiply_convert_fusion = bf16[1024,512]{1,0:T(8,128)(2,1)S(1)} fusion(bf16[2048,512]{1,0:T(8,128)(2,1)S(1)} %copy-done.1, bf16[1024,2048]{1,0:T(8,128)(2,1)} %all-gather.6.cloned.1.call-done, f32[2048]{0:T(1024)S(1)} %convert_element_type.64, f32[1024]{0:T(1024)S(1)} %add_rsqrt_fusion), kind=kOutput, calls=%fused_computation.5 | convolution fusion | flops 2156920832 | bytes 7352320 | tf_op jit(solution)/shard_map/dot_general | solution.py:119
  215.9 0.5 fusion.54
  216.5 8.0 %convolution_convert_fusion = bf16[1024,1024]{1,0:T(8,128)(2,1)S(1)} fusion(bf16[2048,1024]{1,0:T(8,128)(2,1)} %all-gather.10.cloned.1.call-done, bf16[1024,2048]{1,0:T(8,128)(2,1)} %all-gather.6.cloned.1.call-done, f32[2048]{0:T(1024)S(1)} %convert_element_type.64, f32[1024]{0:T(1024)S(1)} %add_rsqrt_fusion), kind=kOutput, calls=%fused_computation.6 | convolution fusion | flops 4304404480 | bytes 10498048 | tf_op jit(solution)/shard_map/dot_general | solution.py:120
  224.6 0.4 fusion.5
  225.0 30.5 %all-gather.1 = f32[64,384]{1,0:T(8,128)S(1)} all-gather(f32[8,384]{1,0:T(8,128)S(1)} %pad_maximum_fusion.2), channel_id=3, replica_groups=mesh['gr'=2,'sp'=8,'tp'=2] {'sp'}, dimensions={0}, use_global_device_ids=true | all-gather | bytes 110592 | tf_op jit(solution)/shard_map/all_gather | solution.py:60
  255.6 0.1 slice_reduce_fusion.2
  255.7 0.2 slice_reduce_fusion.3
  255.8 0.2 exponential_reduce_fusion
  256.3 0.6 fusion.24
  (64 shorter events, 1.3 us)
Async XLA Ops:
  7.2 90.2 %all-gather.8.cloned.1.call-start = ((), (), s32[]{:S(2)}) async-start(), calls=%async_computation.3 | async-start | bytes 2359296 | tf_op jit(solution)/shard_map/all_gather | solution.py:103
  7.9 152.9 %all-gather.10.cloned.1.call-start = ((), (), s32[]{:S(2)}) async-start(), calls=%async_computation.4 | async-start | bytes 4718592 | tf_op jit(solution)/shard_map/all_gather | solution.py:104
  8.6 165.9 %all-gather.6.cloned.1.call-start = ((), (), s32[]{:S(2)}) async-start(), calls=%async_computation.2 | async-start | bytes 6291456 | tf_op jit(solution)/shard_map/all_gather | solution.py:99
  10.5 81.0 %copy-start.5 = (f32[4,256,2,8]{1,3,2,0:T(8,128)S(1)}, f32[4,256,2,8]{1,3,2,0:T(8,128)}, u32[]{:S(2)}) copy-start(f32[4,256,2,8]{1,3,2,0:T(8,128)} %param.19) | copy-start | bytes 196612
  10.5 85.3 %copy-start.6 = (bf16[4,2048]{1,0:T(4,128)(2,1)S(1)}, bf16[4,2048]{1,0:T(4,128)(2,1)}, u32[]{:S(2)}) copy-start(bf16[4,2048]{1,0:T(4,128)(2,1)} %param.11) | copy-start | bytes 49156
  10.5 86.6 %copy-start.9 = (bf16[2048]{0:T(1024)(128)(2,1)S(1)}, bf16[2048]{0:T(1024)(128)(2,1)}, u32[]{:S(2)}) copy-start(bf16[2048]{0:T(1024)(128)(2,1)} %param.13) | copy-start | bytes 12292
  10.5 86.6 %copy-start.10 = (bf16[4,512]{1,0:T(4,128)(2,1)S(1)}, bf16[4,512]{1,0:T(4,128)(2,1)}, u32[]{:S(2)}) copy-start(bf16[4,512]{1,0:T(4,128)(2,1)} %param.12) | copy-start | bytes 12292
  10.5 86.7 %copy-start.7 = (bf16[2048,16]{0,1:T(8,128)(2,1)S(1)}, bf16[2048,16]{0,1:T(8,128)(2,1)}, u32[]{:S(2)}) copy-start(bf16[2048,16]{0,1:T(8,128)(2,1)} %param.17) | copy-start | bytes 196612
  10.5 86.7 %copy-start.8 = (bf16[2048,16]{0,1:T(8,128)(2,1)S(1)}, bf16[2048,16]{0,1:T(8,128)(2,1)}, u32[]{:S(2)}) copy-start(bf16[2048,16]{0,1:T(8,128)(2,1)} %param.16) | copy-start | bytes 196612
  92.2 87.1 %all-to-all-start.1 = ((f32[8,16,128]{2,1,0:T(8,128)}), f32[8,16,128]{2,1,0:T(8,128)S(1)}, u32[]{:S(2)}, u32[]{:S(2)}) async-start(f32[8,16,128]{2,1,0:T(8,128)} %copy.36), calls=%async_computation.1 | async-start | bytes 131072 | tf_op jit(solution)/shard_map/all_to_all | solution.py:101
  174.6 3.4 %copy-start = (bf16[1024,2048]{1,0:T(8,128)(2,1)S(1)}, bf16[1024,2048]{1,0:T(8,128)(2,1)}, u32[]{:S(2)}) copy-start(bf16[1024,2048]{1,0:T(8,128)(2,1)} %all-gather.6.cloned.1.call-done) | copy-start | bytes 12582916
  177.8 1.5 copy-start.11
  178.0 33.3 %copy-start.1 = (bf16[2048,512]{1,0:T(8,128)(2,1)S(1)}, bf16[2048,512]{1,0:T(8,128)(2,1)}, u32[]{:S(2)}) copy-start(bf16[2048,512]{1,0:T(8,128)(2,1)} %all-gather.8.cloned.1.call-done) | copy-start | bytes 6291460
  211.3 4.7 %copy-start.4 = (f32[8,1024]{1,0:T(8,128)}, f32[8,1024]{1,0:T(8,128)S(1)}, u32[]{:S(2)}) copy-start(f32[8,1024]{1,0:T(8,128)S(1)} %get-tuple-element.12) | copy-start | bytes 98308
  215.9 8.6 %copy-start.3 = (bf16[1024,512]{1,0:T(8,128)(2,1)}, bf16[1024,512]{1,0:T(8,128)(2,1)S(1)}, u32[]{:S(2)}) copy-start(bf16[1024,512]{1,0:T(8,128)(2,1)S(1)} %multiply_convert_fusion) | copy-start | bytes 3145732
  224.5 32.4 %copy-start.2 = (bf16[1024,1024]{1,0:T(8,128)(2,1)}, bf16[1024,1024]{1,0:T(8,128)(2,1)S(1)}, u32[]{:S(2)}) copy-start(bf16[1024,1024]{1,0:T(8,128)(2,1)S(1)} %convolution_convert_fusion) | copy-start | bytes 6291460
Sparse Core Ops, SparseCore 0:
  10.1 76.4 all-gather.7
  88.7 72.0 all-gather.9
  162.3 12.1 all-gather.5
where the time goes:
time: 264 us; the launch traced here: 263 us
  blocking collectives  142 us (54%)
  waiting for transfers between devices  73.4 us (28%)
  matrix products  19.9 us (8%)
  between operations  14.8 us (6%)
  other arithmetic  5.59 us (2%)
  local copies, waits for them, and re-layouts  3.73 us (1%)
  starting transfers between devices  3.71 us (1%)
    all_to_all x1, blocking collectives, per_device(): moved = lax.all_to_all(mine, 'sp', split_axis=0, concat_axis=0, tiled=True)  80.9 us
    all_gather x1, waiting for transfers between devices, per_device(): value_weight = lax.all_gather(value_weight, 'sp', axis=0, tiled=True)  61.1 us
    all_gather x1, blocking collectives, log_weights(): everything = lax.all_gather(totals, 'sp')  30.9 us
    all_gather x1, blocking collectives, finish(): lax.all_gather(packed, 'sp').reshape(seq_count, pieces, heads, -1)  30.5 us
    all_gather x1, waiting for transfers between devices, per_device(): source = lax.all_gather(moved.reshape(rows, part), 'tp', axis=1, tiled=True)  10.9 us
    dot_general x2, matrix products, project(): values = jnp.dot(x, value_weight, preferred_element_type=jnp.float32)  10.8 us
    dot_general x2, matrix products, project(): jnp.dot(x, key_weight, preferred_element_type=jnp.float32)  6.53 us
  transfers between devices with their start and end apart: 4, of which 2 were waited for; matrix products, arithmetic and copies ran while one was open for 5% of the time, Pallas kernels for 0%

commit v1 on v0

--- a/solution.py
+++ b/solution.py
@@ -100,8 +100,13 @@
     offsets = jnp.transpose(gate_offsets.reshape(group, sub, 2 * heads), (0, 2, 1))
     offsets = lax.all_to_all(offsets, "sp", split_axis=0, concat_axis=0, tiled=True)
     offsets = jnp.transpose(offsets, (1, 0, 2)).reshape(2 * heads, rows)
-    key_weight = lax.all_gather(key_weight, "sp", axis=0, tiled=True)
-    value_weight = lax.all_gather(value_weight, "sp", axis=0, tiled=True)
+    key_weight, value_weight = jnp.split(
+        lax.all_gather(
+            jnp.concatenate([key_weight, value_weight], axis=1), "sp", axis=0, tiled=True
+        ),
+        [key_weight.shape[1]],
+        axis=1,
+    )
     normed = normed_rows(source, norm_gain)
     fresh = normed_rows(lax.dynamic_slice_in_dim(new_rows, prompt, 1, 0), norm_gain)
     head_start = core * heads

time: 264 us -> 239 us (0.905)
  blocking collectives: 142 us -> 118 us
    all_to_all x1, blocking collectives: 80.9 us -> 55.6 us  [per_device(): moved = lax.all_to_all(mine, 'sp', split_axis=0, concat_axis=0, tiled=True)]
    all_gather x1, waiting for transfers between devices: 10.9 us -> 5.81 us  [per_device(): source = lax.all_gather(moved.reshape(rows, part), 'tp', axis=1, tiled=True)]
    all_gather x2 -> x1, waiting for transfers between devices: 61.1 us -> 65.2 us  [per_device(): lax.all_gather(jnp.concatenate([key_weight, value_weight], axis=1), 'sp',...]
  transfers between devices with their start and end apart: 4 -> 3, of which waited for: 2 -> 2; matrix products, arithmetic and copies ran while one was open for 5% -> 3% of each run, Pallas kernels for 0% -> 0%
where the time goes in v1:
time: 239 us
  blocking collectives  118 us (49%)
  waiting for transfers between devices  71 us (30%)
  matrix products  20.6 us (9%)
  between operations  15.1 us (6%)
  other arithmetic  6.53 us (3%)
  local copies, waits for them, and re-layouts  3.73 us (2%)
  starting transfers between devices  3.67 us (2%)
    all_gather x1, waiting for transfers between devices, per_device(): lax.all_gather(jnp.concatenate([key_weight, value_weight], axis=1), 'sp',...  65.2 us
    all_to_all x1, blocking collectives, per_device(): moved = lax.all_to_all(mine, 'sp', split_axis=0, concat_axis=0, tiled=True)  55.6 us
    all_gather x1, blocking collectives, log_weights(): everything = lax.all_gather(totals, 'sp')  31.9 us
    all_gather x1, blocking collectives, finish(): lax.all_gather(packed, 'sp').reshape(seq_count, pieces, heads, -1)  30.6 us
    dot_general x2, matrix products, project(): values = jnp.dot(x, value_weight, preferred_element_type=jnp.float32)  10.8 us
    dot_general x2, matrix products, project(): jnp.dot(x, key_weight, preferred_element_type=jnp.float32)  7.21 us
    all_gather x1, waiting for transfers between devices, per_device(): source = lax.all_gather(moved.reshape(rows, part), 'tp', axis=1, tiled=True)  5.81 us
  transfers between devices with their start and end apart: 3, of which 2 were waited for; matrix products, arithmetic and copies ran while one was open for 3% of the time, Pallas kernels for 0%

profile of v1, /device:TPU:0, one launch (start us, length us, event | category | flops | bytes accessed | tf_op | source)
XLA Modules:
  0.0 238.7 jit_solution(5324842766984269044)
XLA Ops:
  7.2 1.8 constant_dynamic-slice_fusion.4
  9.1 55.6 %all_to_all.10 = bf16[8,128,1024]{2,1,0:T(8,128)(2,1)} all-to-all(bf16[8,128,1024]{2,1,0:T(8,128)(2,1)S(1)} %constant_dynamic-slice_fusion.4), channel_id=1, replica_groups=mesh['gr'=2,'sp'=8,'tp'=2] {'sp'}, dimensions={0} | all-to-all | bytes 4194304 | tf_op jit(solution)/shard_map/all_to_all | solution.py:98
  64.8 0.9 pad_maximum_fusion
  65.8 0.6 copy.36
  66.5 3.6 %all-to-all-start.1 = ((f32[8,16,128]{2,1,0:T(8,128)}), f32[8,16,128]{2,1,0:T(8,128)S(1)}, u32[]{:S(2)}, u32[]{:S(2)}) async-start(f32[8,16,128]{2,1,0:T(8,128)} %copy.36), calls=%async_computation.1 | async-start | bytes 131072 | tf_op jit(solution)/shard_map/all_to_all | solution.py:101
  70.1 0.6 multiply_reduce_fusion
  71.6 0.1 convolution_bitcast_fusion.1
  71.7 5.8 %all-gather.5.cloned.1.call-done = bf16[1024,2048]{1,0:T(8,128)(2,1)} async-done(((bf16[1024,1024]{1,0:T(8,128)(2,1)}), bf16[1024,2048]{1,0:T(8,128)(2,1)}) %all-gather.5.cloned.1.call-update) | async-done | bytes 4194320 | tf_op jit(solution)/shard_map/all_gather | solution.py:99
  77.5 3.2 %fusion = f32[1024]{0:T(1024)S(1)} fusion(bf16[1024,2048]{1,0:T(8,128)(2,1)} %all-gather.5.cloned.1.call-done), kind=kLoop, calls=%fused_computation.2 | loop fusion | flops 6290432 | bytes 4198400 | tf_op jit(solution)/shard_map/reduce_sum | solution.py:12
  80.8 0.2 copy-done
  81.0 1.3 fusion.22
  82.2 0.2 fusion.63
  82.5 31.9 %all-gather = f32[64,8]{1,0:T(8,128)S(1)} all-gather(f32[8,8]{1,0:T(8,128)S(1)} %copy.38), channel_id=2, replica_groups=mesh['gr'=2,'sp'=8,'tp'=2] {'sp'}, dimensions={0}, use_global_device_ids=true | all-gather | bytes 2304 | tf_op jit(solution)/shard_map/all_gather | solution.py:30
  114.6 0.1 multiply_reduce_fusion.1
  114.8 0.3 fusion.17
  115.0 0.1 fusion.61
  115.2 0.1 copy.41
  115.2 65.2 %all-gather.7.cloned.1.call-done = bf16[2048,1536]{1,0:T(8,128)(2,1)} async-done(((bf16[256,1536]{1,0:T(8,128)(2,1)}), bf16[2048,1536]{1,0:T(8,128)(2,1)}) %all-gather.7.cloned.1.call-update) | async-done | bytes 6291472 | tf_op jit(solution)/shard_map/all_gather | solution.py:104
  180.4 2.8 %fusion.3 = f32[1,1024]{1,0:T(1,128)S(1)} fusion(bf16[2048,1536]{1,0:T(8,128)(2,1)} %all-gather.7.cloned.1.call-done, bf16[1,2048]{1,0:T(2,128)(2,1)S(1)} %multiply_multiply_fusion), kind=kOutput, calls=%fused_computation.5 | convolution fusion | flops 4194304 | bytes 4202496 | tf_op jit(solution)/shard_map/dot_general | solution.py:125
  183.3 2.0 fusion.10
  185.4 0.1 reduce_sum.99
  185.5 0.1 copy.43
  185.6 5.2 %multiply_convert_fusion = bf16[1024,512]{1,0:T(8,128)(2,1)S(1)} fusion(bf16[2048,1536]{1,0:T(8,128)(2,1)} %all-gather.7.cloned.1.call-done, bf16[1024,2048]{1,0:T(8,128)(2,1)} %all-gather.5.cloned.1.call-done, f32[2048]{0:T(1024)S(1)} %convert_element_type.64, f32[1024]{0:T(1024)S(1)} %add_rsqrt_fusion), kind=kOutput, calls=%fused_computation.9 | convolution fusion | flops 2156920832 | bytes 7352320 | tf_op jit(solution)/shard_map/dot_general | solution.py:124
  190.9 0.5 fusion.65
  191.3 0.1 copy.42
  191.4 8.0 %fusion.7 = bf16[1024,1024]{1,0:T(8,128)(2,1)S(1)} fusion(bf16[2048,1536]{1,0:T(8,128)(2,1)} %all-gather.7.cloned.1.call-done, bf16[1024,2048]{1,0:T(8,128)(2,1)} %all-gather.5.cloned.1.call-done, f32[2048]{0:T(1024)S(1)} %convert_element_type.64, f32[1024]{0:T(1024)S(1)} %add_rsqrt_fusion), kind=kOutput, calls=%fused_computation.10 | convolution fusion | flops 4304404480 | bytes 10498048 | tf_op jit(solution)/shard_map/dot_general | solution.py:125
  199.5 0.4 fusion.18
  199.9 30.6 %all-gather.1 = f32[64,384]{1,0:T(8,128)S(1)} all-gather(f32[8,384]{1,0:T(8,128)S(1)} %pad_maximum_fusion.3), channel_id=3, replica_groups=mesh['gr'=2,'sp'=8,'tp'=2] {'sp'}, dimensions={0}, use_global_device_ids=true | all-gather | bytes 110592 | tf_op jit(solution)/shard_map/all_gather | solution.py:60
  230.5 0.1 slice_reduce_fusion.2
  230.6 0.2 slice_reduce_fusion.3
  230.8 0.2 exponential_reduce_fusion
  231.2 0.6 fusion.37
  (64 shorter events, 1.2 us)
Async XLA Ops:
  7.2 70.4 %all-gather.5.cloned.1.call-start = ((), (), s32[]{:S(2)}) async-start(), calls=%async_computation.2 | async-start | bytes 6291456 | tf_op jit(solution)/shard_map/all_gather | solution.py:99
  9.0 55.8 %copy-start.3 = (bf16[256,1024]{1,0:T(8,128)(2,1)S(1)}, bf16[256,1024]{1,0:T(8,128)(2,1)}, u32[]{:S(2)}) copy-start(bf16[256,1024]{1,0:T(8,128)(2,1)} %param.15) | copy-start | bytes 1572868
  9.0 55.8 %copy-start.4 = (bf16[256,512]{1,0:T(8,128)(2,1)S(1)}, bf16[256,512]{1,0:T(8,128)(2,1)}, u32[]{:S(2)}) copy-start(bf16[256,512]{1,0:T(8,128)(2,1)} %param.14) | copy-start | bytes 786436
  9.0 56.7 %copy-start.6 = (f32[4,256,2,8]{1,3,2,0:T(8,128)S(1)}, f32[4,256,2,8]{1,3,2,0:T(8,128)}, u32[]{:S(2)}) copy-start(f32[4,256,2,8]{1,3,2,0:T(8,128)} %param.19) | copy-start | bytes 196612
  9.0 61.0 %copy-start.7 = (bf16[4,2048]{1,0:T(4,128)(2,1)S(1)}, bf16[4,2048]{1,0:T(4,128)(2,1)}, u32[]{:S(2)}) copy-start(bf16[4,2048]{1,0:T(4,128)(2,1)} %param.11) | copy-start | bytes 49156
  9.0 62.3 %copy-start.10 = (bf16[2048]{0:T(1024)(128)(2,1)S(1)}, bf16[2048]{0:T(1024)(128)(2,1)}, u32[]{:S(2)}) copy-start(bf16[2048]{0:T(1024)(128)(2,1)} %param.13) | copy-start | bytes 12292
  9.0 62.4 %copy-start.11 = (bf16[4,512]{1,0:T(4,128)(2,1)S(1)}, bf16[4,512]{1,0:T(4,128)(2,1)}, u32[]{:S(2)}) copy-start(bf16[4,512]{1,0:T(4,128)(2,1)} %param.12) | copy-start | bytes 12292
  9.1 62.4 %copy-start.8 = (bf16[2048,16]{0,1:T(8,128)(2,1)S(1)}, bf16[2048,16]{0,1:T(8,128)(2,1)}, u32[]{:S(2)}) copy-start(bf16[2048,16]{0,1:T(8,128)(2,1)} %param.17) | copy-start | bytes 196612
  9.1 62.4 %copy-start.9 = (bf16[2048,16]{0,1:T(8,128)(2,1)S(1)}, bf16[2048,16]{0,1:T(8,128)(2,1)}, u32[]{:S(2)}) copy-start(bf16[2048,16]{0,1:T(8,128)(2,1)} %param.16) | copy-start | bytes 196612
  64.7 115.8 %all-gather.7.cloned.1.call-start = ((), (), s32[]{:S(2)}) async-start(), calls=%async_computation.3 | async-start | bytes 7077888 | tf_op jit(solution)/shard_map/all_gather | solution.py:104
  66.5 15.8 %all-to-all-start.1 = ((f32[8,16,128]{2,1,0:T(8,128)}), f32[8,16,128]{2,1,0:T(8,128)S(1)}, u32[]{:S(2)}, u32[]{:S(2)}) async-start(f32[8,16,128]{2,1,0:T(8,128)} %copy.36), calls=%async_computation.1 | async-start | bytes 131072 | tf_op jit(solution)/shard_map/all_to_all | solution.py:101
  77.5 3.4 %copy-start = (bf16[1024,2048]{1,0:T(8,128)(2,1)S(1)}, bf16[1024,2048]{1,0:T(8,128)(2,1)}, u32[]{:S(2)}) copy-start(bf16[1024,2048]{1,0:T(8,128)(2,1)} %all-gather.5.cloned.1.call-done) | copy-start | bytes 12582916
  80.7 1.5 copy-start.12
  115.2 75.7 %copy-start.5 = (f32[8,1024]{1,0:T(8,128)}, f32[8,1024]{1,0:T(8,128)S(1)}, u32[]{:S(2)}) copy-start(f32[8,1024]{1,0:T(8,128)S(1)} %get-tuple-element.12) | copy-start | bytes 98308
  190.8 8.6 %copy-start.2 = (bf16[1024,512]{1,0:T(8,128)(2,1)}, bf16[1024,512]{1,0:T(8,128)(2,1)S(1)}, u32[]{:S(2)}) copy-start(bf16[1024,512]{1,0:T(8,128)(2,1)S(1)} %multiply_convert_fusion) | copy-start | bytes 3145732
  199.5 32.4 %copy-start.1 = (bf16[1024,1024]{1,0:T(8,128)(2,1)}, bf16[1024,1024]{1,0:T(8,128)(2,1)S(1)}, u32[]{:S(2)}) copy-start(bf16[1024,1024]{1,0:T(8,128)(2,1)S(1)} %fusion.7) | copy-start | bytes 6291460
Sparse Core Ops, SparseCore 0:
  64.8 12.6 all-gather.4
  80.3 100.1 all-gather.6
